TPU v7x, 32 devices: a whole 2x2x4 slice. The times are simulated.
32 devices in a mesh: fs: 4 (over z), rep: 4 (over y, x), tp: 2 (over core).
Axes of the slice: x: 2, y: 2, z: 4, core: 2. Of those that a mesh axis runs over, the one named last changes fastest.
Arguments:
- first_mix: bfloat16 [12288, 2048], P(('fs', 'rep'), 'tp'), may hold values from -6 to 6
- second_mix: bfloat16 [12288, 2048], P(('fs', 'rep'), 'tp'), may hold values from -6 to 6
- lambda_head: float32 [8], P('tp'), may hold values from 0.3 to 0.8
- head_gain: float32 [256], replicated, may hold values from 0.1 to 1.9
- out_cotangent: bfloat16 [12288, 2048], P(('fs', 'rep')), may hold values from -0.053955078 to 0.053955078
- basis: bfloat16 [2048, 256], P('tp'), may hold values from -0.125 to 0.125
- weight: float32 [2048, 2048], P('tp', 'fs'), may hold values from -3 to 3
- first_moment: float32 [2048, 256], P('fs', 'tp'), may hold values from -4.5 to 4.5
- second_moment: float32 [2048, 256], P('fs', 'tp'), may hold values from 0.05 to 0.5
Outputs:
- weight_new: float32 [2048, 2048], P('tp', 'fs')
- weight_copy: bfloat16 [2048, 2048], P('tp')
- step_out: float32 [2048, 2048], P('tp', 'fs')
- first_new: float32 [2048, 256], P('fs', 'tp')
- second_new: float32 [2048, 256], P('fs', 'tp')
All inputs are finite; a program needn't handle non-finite values.
Results may differ from a plain program's by a relative error of at most 0.0075.
Values may be sent and summed in bfloat16 or wider, within the bound.
A program may use at most 64 MiB of HBM per device.

v0:
```python
import jax
import jax.numpy as jnp
from jax import lax
from jax.sharding import PartitionSpec as P

out_scale = 0.8
beta_first = 0.9
beta_second = 0.95


def head_output(first_piece, second_piece, lambdas, head_gain):
    token_count = first_piece.shape[0]
    head_width = head_gain.shape[0]
    head_count = lambdas.shape[0] // head_width
    mixture = first_piece.astype(jnp.float32) - lambdas[None, :] * second_piece.astype(jnp.float32)
    grouped = mixture.reshape(token_count, head_count, head_width)
    inverse = lax.rsqrt(jnp.mean(grouped * grouped, axis=-1, keepdims=True) + 1e-06)
    normed = grouped * inverse * head_gain[None, None, :] * out_scale
    return normed.reshape(token_count, head_count * head_width).astype(jnp.bfloat16)


def split_product(narrow, wide, numbers):
    upper = wide.astype(jnp.bfloat16)
    lower = (wide - upper.astype(jnp.float32)).astype(jnp.bfloat16)
    return lax.dot_general(
        narrow, upper, numbers, preferred_element_type=jnp.float32
    ) + lax.dot_general(narrow, lower, numbers, preferred_element_type=jnp.float32)


def body(
    first_mix,
    second_mix,
    lambda_head,
    head_gain,
    out_cotangent,
    basis,
    weight,
    first_moment,
    second_moment,
):
    lambdas = jnp.repeat(lambda_head, head_gain.shape[0])
    head_out = head_output(first_mix, second_mix, lambdas, head_gain)
    reduced = jnp.dot(head_out, basis, preferred_element_type=jnp.float32)
    proj_rows = lax.psum_scatter(
        split_product(out_cotangent, reduced, (((0,), (0,)), ((), ()))),
        "fs",
        scatter_dimension=0,
        tiled=True,
    )
    proj_rows = lax.psum_scatter(proj_rows, "tp", scatter_dimension=1, tiled=True)
    projected = lax.psum(proj_rows, "rep")
    first_new = beta_first * first_moment + (1.0 - beta_first) * projected
    second_new = beta_second * second_moment + (1.0 - beta_second) * projected * projected
    direction = first_new / (jnp.sqrt(second_new) + 1e-08)
    energy = lax.psum(jnp.sum(direction * direction), ("fs", "tp"))
    entries = direction.shape[0] * direction.shape[1] * lax.axis_size("fs") * lax.axis_size("tp")
    spread = jnp.sqrt(energy / entries)
    full_direction = lax.all_gather(direction, "tp", axis=1, tiled=True)
    step_out = split_product(basis, full_direction, (((1,), (1,)), ((), ()))) * (
        -1.0 / (spread + 1e-06)
    )
    weight_new = weight + step_out
    weight_copy = lax.all_gather(weight_new.astype(jnp.bfloat16), "fs", axis=1, tiled=True)
    return (weight_new, weight_copy, step_out, first_new, second_new)


def solution(mesh):
    return jax.shard_map(
        body,
        mesh=mesh,
        in_specs=(
            P(("fs", "rep"), "tp"),
            P(("fs", "rep"), "tp"),
            P("tp"),
            P(),
            P(("fs", "rep"), None),
            P("tp", None),
            P("tp", "fs"),
            P("fs", "tp"),
            P("fs", "tp"),
        ),
        out_specs=(P("tp", "fs"), P("tp", None), P("tp", "fs"), P("fs", "tp"), P("fs", "tp")),
        check_vma=False,
    )
```

profile of v0, /device:TPU:0, one launch (start us, length us, event | category | flops | bytes accessed | tf_op | source)
XLA Modules:
  0.0 254.0 jit_solution(11689265764747644795)
XLA Ops:
  7.2 0.0 copy-start
  7.2 0.0 reduce-scatter.3.cloned.1.call-start
  7.2 0.9 broadcast_bitcast_fusion.1
  8.1 0.7 broadcast_bitcast_fusion
  8.8 4.2 %fusion = f32[768,1024]{1,0:T(8,128)} fusion(bf16[768,1024]{1,0:T(8,128)(2,1)} %param.10, bf16[768,1024]{1,0:T(8,128)(2,1)} %param.9, f32[1024]{0:T(1024)S(1)} %bitcast.19), kind=kLoop, calls=%fused_computation.2 | loop fusion | flops 3932160 | bytes 6295552 | tf_op jit(solution)/shard_map/mul | solution.py:17
  13.0 5.2 %mul.92 = f32[768,4,256]{2,1,0:T(4,128)} reshape(f32[768,1024]{1,0:T(8,128)} %fusion) | data formatting | bytes 6291456 | tf_op jit(solution)/shard_map/mul | solution.py:17
  18.2 2.8 %reduce_sum.18 = f32[768,4]{1,0:T(8,128)S(1)} reduce(f32[768,4,256]{2,1,0:T(4,128)} %mul.92, f32[]{:T(128)} %constant.2.clone.1), dimensions={2}, to_apply=%region_0.0 | reduce | flops 783360 | bytes 3158020 | tf_op jit(solution)/shard_map/reduce_sum | solution.py:17
  21.0 0.1 add_rsqrt_fusion
  21.1 1.0 mul.93
  22.0 0.0 copy-start.1
  22.1 0.0 copy-start.2
  22.1 0.0 copy-start.3
  22.1 0.8 copy.42
  22.8 0.6 copy-done.1
  23.5 0.5 copy-done.2
  23.9 0.1 copy-done.3
  24.0 0.9 fusion.2
  25.0 0.0 copy-done
  25.0 1.0 fusion.5
  26.0 0.0 copy-start.6
  26.0 2.4 fusion.1
  28.4 0.0 reduce-scatter.3.cloned.1.call-update
  28.4 0.0 reduce-scatter.5.cloned.1.call-start
  28.5 46.5 %reduce-scatter.3.cloned.1.call-done = f32[512,256]{0,1:T(8,128)} async-done(((f32[2048,256]{0,1:T(8,128)}), f32[512,256]{0,1:T(8,128)}) %reduce-scatter.3.cloned.1.call-update) | async-done | bytes 524304 | tf_op jit(solution)/shard_map/reduce_scatter | solution.py:44
  74.9 0.0 reduce-scatter.5.cloned.1.call-update
  74.9 0.0 all-reduce.2.cloned.1.call-start
  75.0 9.3 %reduce-scatter.5.cloned.1.call-done = f32[512,128]{0,1:T(8,128)} async-done(((f32[512,256]{0,1:T(8,128)}), f32[512,128]{0,1:T(8,128)}) %reduce-scatter.5.cloned.1.call-update) | async-done | bytes 262160 | tf_op jit(solution)/shard_map/reduce_scatter | solution.py:50
  84.3 0.0 all-reduce.2.cloned.1.call-update
  84.4 0.0 all-gather.2.cloned.1.call-start
  84.4 0.0 copy-done.6
  84.4 0.8 copy.31
  85.2 1.8 copy.34
  87.0 2.9 %copy.35 = f32[1024,512]{0,1:T(8,128)} copy(f32[1024,512]{1,0:T(8,128)} %param.15) | data formatting | bytes 4194304 | tf_op args[6]
  89.9 41.6 %all-reduce.2.cloned.1.call-done = f32[512,128]{0,1:T(8,128)} async-done(((f32[512,128]{0,1:T(8,128)}), f32[512,128]{0,1:T(8,128)}) %all-reduce.2.cloned.1.call-update) | async-done | bytes 262160 | tf_op jit(solution)/shard_map/psum | solution.py:51
  131.5 2.6 %multiply_reduce_fusion = (f32[]{:T(128)}, f32[512,128]{0,1:T(8,128)S(1)}, f32[512,128]{0,1:T(8,128)}, f32[512,128]{0,1:T(8,128)}) fusion(f32[512,128]{0,1:T(8,128)} %all-reduce.2.cloned.1.call-done, f32[512,128]{0,1:T(8,128)} %copy.34, f32[512,128]{0,1:T(8,128)} %copy.31), kind=kLoop, calls=%fused_computation.12 | loop fusion | flops 720895 | bytes 1572868 | tf_op jit(solution)/shard_map/reduce_sum | solution.py:55
  134.1 16.5 %psum.15 = f32[]{:T(128)} all-reduce(f32[]{:T(128)} %get-tuple-element.22), channel_id=1, replica_groups=mesh['fs'=4,'rep'=4,'tp'=2] {'fs','tp'}, use_global_device_ids=true, to_apply=%region_5.0 | all-reduce | flops 1 | bytes 8 | tf_op jit(solution)/shard_map/psum | solution.py:55
  151.3 2.2 all_gather.6
  153.5 0.8 copy-done.4
  154.3 2.8 %fusion.8 = f32[512,1024]{1,0:T(8,128)} fusion(bf16[1024,256]{1,0:T(8,128)(2,1)} %param.14, f32[512,256]{0,1:T(8,128)S(1)} %all_gather.6), kind=kOutput, calls=%fused_computation.19 | convolution fusion | flops 268566528 | bytes 3145728 | tf_op jit(solution)/shard_map/dot_general | solution.py:25
  157.2 0.0 copy-start.5
  157.2 5.7 %fusion.11 = (bf16[1024,512]{0,1:T(8,128)(2,1)}, f32[1024,512]{0,1:T(8,128)}, f32[1024,512]{0,1:T(8,128)}) fusion(f32[1024,512]{0,1:T(8,128)} %copy.35, f32[]{:T(128)S(6)} %div.19, f32[512,1024]{1,0:T(8,128)} %fusion.8, bf16[1024,256]{1,0:T(8,128)(2,1)} %param.14, f32[512,256]{0,1:T(8,128)} %copy-done.4), kind=kOutput, calls=%fused_computation.24 | convolution fusion | flops 271056896 | bytes 10485764 | tf_op jit(solution)/shard_map/dot_general | solution.py:27
  162.9 0.0 all-gather.2.cloned.1.call-update
  162.9 1.8 copy.40
  164.7 0.8 copy.39
  165.5 3.0 %copy.36 = f32[1024,512]{1,0:T(8,128)} copy(f32[1024,512]{0,1:T(8,128)} %get-tuple-element.21) | data formatting | bytes 4194304
  168.5 3.0 %copy.38 = f32[1024,512]{1,0:T(8,128)} copy(f32[1024,512]{0,1:T(8,128)} %get-tuple-element.26) | data formatting | bytes 4194304
  171.5 69.5 %all-gather.2.cloned.1.call-done = bf16[1024,2048]{0,1:T(8,128)(2,1)} async-done(((bf16[1024,512]{0,1:T(8,128)(2,1)}), bf16[1024,2048]{0,1:T(8,128)(2,1)}) %all-gather.2.cloned.1.call-update) | async-done | bytes 4194320 | tf_op jit(solution)/shard_map/all_gather | solution.py:63
  241.0 6.4 %copy.37 = bf16[1024,2048]{1,0:T(8,128)(2,1)} copy(bf16[1024,2048]{0,1:T(8,128)(2,1)} %all-gather.2.cloned.1.call-done) | data formatting | bytes 8388608
  (4 shorter events, 0.0 us)
Async XLA Ops:
  7.2 17.8 %copy-start = (bf16[768,2048]{1,0:T(8,128)(2,1)S(1)}, bf16[768,2048]{1,0:T(8,128)(2,1)}, u32[]{:S(2)}) copy-start(bf16[768,2048]{1,0:T(8,128)(2,1)} %param.13) | copy-start | bytes 9437188
  7.2 67.7 %reduce-scatter.3.cloned.1.call-start = ((), (), s32[]{:S(2)}) async-start(), calls=%async_computation.2 | async-start | bytes 2621440 | tf_op jit(solution)/shard_map/reduce_scatter | solution.py:44
  22.0 1.4 copy-start.1
  22.1 1.9 copy-start.2
  22.1 2.0 copy-start.3
  26.0 58.4 %copy-start.6 = (f32[512,128]{1,0:T(8,128)S(1)}, f32[512,128]{1,0:T(8,128)}, u32[]{:S(2)}) copy-start(f32[512,128]{1,0:T(8,128)} %param.16) | copy-start | bytes 786436
  28.4 55.9 %reduce-scatter.5.cloned.1.call-start = ((), (), s32[]{:S(2)}) async-start(), calls=%async_computation.3 | async-start | bytes 786432 | tf_op jit(solution)/shard_map/reduce_scatter | solution.py:50
  74.9 56.5 %all-reduce.2.cloned.1.call-start = ((), (), s32[]{:S(2)}) async-start(), calls=%async_computation.4 | async-start | bytes 524288 | tf_op jit(solution)/shard_map/psum | solution.py:51
  84.4 156.6 %all-gather.2.cloned.1.call-start = ((), (), s32[]{:S(2)}) async-start(), calls=%async_computation.5 | async-start | bytes 5242880 | tf_op jit(solution)/shard_map/all_gather | solution.py:63
  153.5 0.8 copy-start.4
  157.2 7.5 %copy-start.5 = (f32[512,128]{0,1:T(8,128)S(1)}, f32[512,128]{0,1:T(8,128)}, u32[]{:S(2)}) copy-start(f32[512,128]{0,1:T(8,128)} %get-tuple-element.25) | copy-start | bytes 786436
Sparse Core Ops, SparseCore 0:
  28.5 46.3 reduce-scatter.2
  77.2 7.1 reduce-scatter.4
  87.3 44.1 all-reduce.1
  163.0 77.9 all-gather.1
where the time goes:
time: 255 us; the launch traced here: 254 us
  waiting for transfers between devices  167 us (65%)
  local copies, waits for them, and re-layouts  31 us (12%)
  blocking collectives  18.7 us (7%)
  between operations  14.6 us (6%)
  matrix products  12.8 us (5%)
  other arithmetic  9.72 us (4%)
    all_gather x1, waiting for transfers between devices, body(): lax.all_gather(weight_new.astype(jnp.bfloat16), 'fs', axis=1, tiled=True)  69.5 us
    reduce_scatter x1, waiting for transfers between devices, body(): lax.psum_scatter(split_product(out_cotangent, reduced, (((0,), (0,)), (()...  46.5 us
    psum x1, waiting for transfers between devices, body(): projected = lax.psum(proj_rows, 'rep')  41.6 us
    unnamed x27, local copies, waits for them, and re-layouts  24.9 us
    psum x1, blocking collectives, body(): energy = lax.psum(jnp.sum(direction * direction), ('fs', 'tp'))  16.5 us
    reduce_scatter x1, waiting for transfers between devices, body(): lax.psum_scatter(proj_rows, 'tp', scatter_dimension=1, tiled=True)  9.34 us
    dot_general x2, matrix products, split_product(): lax.dot_general(narrow, lower, numbers, preferred_element_type=jnp.float32)  8.03 us
    mul x1, local copies, waits for them, and re-layouts, head_output(): grouped * grouped  5.15 us
  transfers between devices with their start and end apart: 4, of which 4 were waited for; matrix products, arithmetic and copies ran while one was open for 6% of the time, Pallas kernels for 0%

commit v1 on v0

--- a/solution.py
+++ b/solution.py
@@ -60,7 +60,7 @@
         -1.0 / (spread + 1e-06)
     )
     weight_new = weight + step_out
-    weight_copy = lax.all_gather(weight_new.astype(jnp.bfloat16), "fs", axis=1, tiled=True)
+    weight_copy = jnp.concatenate(lax.all_gather(weight_new.astype(jnp.bfloat16), "fs"), axis=1)
     return (weight_new, weight_copy, step_out, first_new, second_new)
 
 

time: 255 us -> 272 us (1.067)
  local copies, waits for them, and re-layouts: 31 us -> 48.2 us
    reshape x0 -> x1, local copies, waits for them, and re-layouts: none -> 10.2 us  [body(): jnp.concatenate(lax.all_gather(weight_new.astype(jnp.bfloat16), 'fs'), ax...]
    all_gather x0 -> x1, local copies, waits for them, and re-layouts: none -> 7.82 us  [body(): lax.all_gather(weight_new.astype(jnp.bfloat16), 'fs')]
  transfers between devices with their start and end apart: 4 -> 4, of which waited for: 4 -> 4; matrix products, arithmetic and copies ran while one was open for 6% -> 5% of each run, Pallas kernels for 0% -> 0%
where the time goes in v1:
time: 272 us; the launch traced here: 271 us
  waiting for transfers between devices  167 us (61%)
  local copies, waits for them, and re-layouts  48.2 us (18%)
  blocking collectives  18.7 us (7%)
  between operations  14.6 us (5%)
  matrix products  12.8 us (5%)
  other arithmetic  9.72 us (4%)
    all_gather x1, waiting for transfers between devices, body(): lax.all_gather(weight_new.astype(jnp.bfloat16), 'fs')  69.5 us
    reduce_scatter x1, waiting for transfers between devices, body(): lax.psum_scatter(split_product(out_cotangent, reduced, (((0,), (0,)), (()...  46.5 us
    psum x1, waiting for transfers between devices, body(): projected = lax.psum(proj_rows, 'rep')  41.6 us
    unnamed x27, local copies, waits for them, and re-layouts  24 us
    psum x1, blocking collectives, body(): energy = lax.psum(jnp.sum(direction * direction), ('fs', 'tp'))  16.5 us
    reshape x1, local copies, waits for them, and re-layouts, body(): jnp.concatenate(lax.all_gather(weight_new.astype(jnp.bfloat16), 'fs'), ax...  10.2 us
    reduce_scatter x1, waiting for transfers between devices, body(): lax.psum_scatter(proj_rows, 'tp', scatter_dimension=1, tiled=True)  9.34 us
    dot_general x2, matrix products, split_product(): lax.dot_general(narrow, lower, numbers, preferred_element_type=jnp.float32)  8.03 us
  transfers between devices with their start and end apart: 4, of which 4 were waited for; matrix products, arithmetic and copies ran while one was open for 5% of the time, Pallas kernels for 0%

profile of v1, /device:TPU:0, one launch (start us, length us, event | category | flops | bytes accessed | tf_op | source)
XLA Modules:
  0.0 271.1 jit_solution(3114219503058571143)
XLA Ops:
  7.2 0.0 copy-start
  7.2 0.0 reduce-scatter.3.cloned.1.call-start
  7.2 0.9 broadcast_bitcast_fusion.1
  8.1 0.7 broadcast_bitcast_fusion
  8.8 4.2 %fusion = f32[768,1024]{1,0:T(8,128)} fusion(bf16[768,1024]{1,0:T(8,128)(2,1)} %param.10, bf16[768,1024]{1,0:T(8,128)(2,1)} %param.9, f32[1024]{0:T(1024)S(1)} %bitcast.27), kind=kLoop, calls=%fused_computation.2 | loop fusion | flops 3932160 | bytes 6295552 | tf_op jit(solution)/shard_map/mul | solution.py:17
  13.0 5.2 %mul.92 = f32[768,4,256]{2,1,0:T(4,128)} reshape(f32[768,1024]{1,0:T(8,128)} %fusion) | data formatting | bytes 6291456 | tf_op jit(solution)/shard_map/mul | solution.py:17
  18.2 2.8 %reduce_sum.18 = f32[768,4]{1,0:T(8,128)S(1)} reduce(f32[768,4,256]{2,1,0:T(4,128)} %mul.92, f32[]{:T(128)} %constant.2.clone.1), dimensions={2}, to_apply=%region_0.0 | reduce | flops 783360 | bytes 3158020 | tf_op jit(solution)/shard_map/reduce_sum | solution.py:17
  21.0 0.1 add_rsqrt_fusion
  21.1 1.0 mul.93
  22.0 0.0 copy-start.1
  22.1 0.0 copy-start.2
  22.1 0.0 copy-start.3
  22.1 0.8 copy.42
  22.8 0.6 copy-done.1
  23.5 0.5 copy-done.2
  23.9 0.1 copy-done.3
  24.0 0.9 fusion.2
  25.0 0.0 copy-done
  25.0 1.0 fusion.5
  26.0 0.0 copy-start.6
  26.0 2.4 fusion.1
  28.4 0.0 reduce-scatter.3.cloned.1.call-update
  28.4 0.0 reduce-scatter.5.cloned.1.call-start
  28.5 46.5 %reduce-scatter.3.cloned.1.call-done = f32[512,256]{0,1:T(8,128)} async-done(((f32[2048,256]{0,1:T(8,128)}), f32[512,256]{0,1:T(8,128)}) %reduce-scatter.3.cloned.1.call-update) | async-done | bytes 524304 | tf_op jit(solution)/shard_map/reduce_scatter | solution.py:44
  74.9 0.0 reduce-scatter.5.cloned.1.call-update
  74.9 0.0 all-reduce.2.cloned.1.call-start
  75.0 9.3 %reduce-scatter.5.cloned.1.call-done = f32[512,128]{0,1:T(8,128)} async-done(((f32[512,256]{0,1:T(8,128)}), f32[512,128]{0,1:T(8,128)}) %reduce-scatter.5.cloned.1.call-update) | async-done | bytes 262160 | tf_op jit(solution)/shard_map/reduce_scatter | solution.py:50
  84.3 0.0 all-reduce.2.cloned.1.call-update
  84.4 0.0 all-gather.3.cloned.1.call-start
  84.4 0.8 copy.31
  85.2 1.8 copy.34
  87.0 2.9 %copy.35 = f32[1024,512]{0,1:T(8,128)} copy(f32[1024,512]{1,0:T(8,128)} %param.15) | data formatting | bytes 4194304 | tf_op args[6]
  89.9 41.6 %all-reduce.2.cloned.1.call-done = f32[512,128]{0,1:T(8,128)} async-done(((f32[512,128]{0,1:T(8,128)}), f32[512,128]{0,1:T(8,128)}) %all-reduce.2.cloned.1.call-update) | async-done | bytes 262160 | tf_op jit(solution)/shard_map/psum | solution.py:51
  131.5 2.6 multiply_reduce_fusion
  134.1 16.5 %psum.15 = f32[]{:T(128)} all-reduce(f32[]{:T(128)} %get-tuple-element.22), channel_id=1, replica_groups=mesh['fs'=4,'rep'=4,'tp'=2] {'fs','tp'}, use_global_device_ids=true, to_apply=%region_5.0 | all-reduce | flops 1 | bytes 8 | tf_op jit(solution)/shard_map/psum | solution.py:55
  151.3 2.2 all_gather.9
  153.5 0.8 copy-done.4
  154.3 2.8 %fusion.8 = f32[512,1024]{1,0:T(8,128)} fusion(bf16[1024,256]{1,0:T(8,128)(2,1)} %param.14, f32[512,256]{0,1:T(8,128)S(1)} %all_gather.9), kind=kOutput, calls=%fused_computation.19 | convolution fusion | flops 268566528 | bytes 3145728 | tf_op jit(solution)/shard_map/dot_general | solution.py:25
  157.2 5.7 %fusion.11 = (bf16[1024,512]{0,1:T(8,128)(2,1)}, f32[1024,512]{0,1:T(8,128)}, f32[1024,512]{0,1:T(8,128)}) fusion(f32[1024,512]{0,1:T(8,128)} %copy.35, f32[]{:T(128)S(6)} %div.19, f32[512,1024]{1,0:T(8,128)} %fusion.8, bf16[1024,256]{1,0:T(8,128)(2,1)} %param.14, f32[512,256]{0,1:T(8,128)} %copy-done.4), kind=kOutput, calls=%fused_computation.24 | convolution fusion | flops 271056896 | bytes 10485764 | tf_op jit(solution)/shard_map/dot_general | solution.py:27
  162.9 0.0 all-gather.3.cloned.1.call-update
  162.9 1.8 copy.40
  164.7 0.8 copy.39
  165.5 3.0 %copy.37 = f32[1024,512]{1,0:T(8,128)} copy(f32[1024,512]{0,1:T(8,128)} %get-tuple-element.21) | data formatting | bytes 4194304
  168.5 3.0 %copy.38 = f32[1024,512]{1,0:T(8,128)} copy(f32[1024,512]{0,1:T(8,128)} %get-tuple-element.26) | data formatting | bytes 4194304
  171.5 69.5 %all-gather.3.cloned.1.call-done = bf16[4096,512]{0,1:T(8,128)(2,1)} async-done(((bf16[1024,512]{0,1:T(8,128)(2,1)}), bf16[4096,512]{0,1:T(8,128)(2,1)}) %all-gather.3.cloned.1.call-update) | async-done | bytes 4194320 | tf_op jit(solution)/shard_map/all_gather | solution.py:63
  241.0 7.8 %reshape.33 = bf16[4,1024,512]{1,0,2:T(4,128)(2,1)} reshape(bf16[4096,512]{0,1:T(8,128)(2,1)} %all-gather.3.cloned.1.call-done) | data formatting | bytes 8388608 | tf_op jit(solution)/shard_map/all_gather | solution.py:63
  248.8 10.2 %copy.36 = bf16[1024,4,512]{2,1,0:T(4,128)(2,1)} copy(bf16[1024,4,512]{0,1,2:T(4,128)(2,1)} %bitcast.22) | data formatting | bytes 8388608 | tf_op jit(solution)/shard_map/reshape | solution.py:63
  259.0 5.6 %copy.44 = bf16[128,8,4,512]{3,1,2,0:T(8,128)(2,1)} copy(bf16[128,8,4,512]{3,2,1,0:T(4,128)(2,1)} %bitcast.23) | data formatting | bytes 8388608
  (6 shorter events, 0.0 us)
Async XLA Ops:
  7.2 17.8 %copy-start = (bf16[768,2048]{1,0:T(8,128)(2,1)S(1)}, bf16[768,2048]{1,0:T(8,128)(2,1)}, u32[]{:S(2)}) copy-start(bf16[768,2048]{1,0:T(8,128)(2,1)} %param.13) | copy-start | bytes 9437188
  7.2 67.7 %reduce-scatter.3.cloned.1.call-start = ((), (), s32[]{:S(2)}) async-start(), calls=%async_computation.2 | async-start | bytes 2621440 | tf_op jit(solution)/shard_map/reduce_scatter | solution.py:44
  22.0 1.4 copy-start.1
  22.1 1.9 copy-start.2
  22.1 2.0 copy-start.3
  26.0 58.4 %copy-start.6 = (f32[512,128]{1,0:T(8,128)S(1)}, f32[512,128]{1,0:T(8,128)}, u32[]{:S(2)}) copy-start(f32[512,128]{1,0:T(8,128)} %param.16) | copy-start | bytes 786436
  28.4 55.9 %reduce-scatter.5.cloned.1.call-start = ((), (), s32[]{:S(2)}) async-start(), calls=%async_computation.3 | async-start | bytes 786432 | tf_op jit(solution)/shard_map/reduce_scatter | solution.py:50
  74.9 56.5 %all-reduce.2.cloned.1.call-start = ((), (), s32[]{:S(2)}) async-start(), calls=%async_computation.4 | async-start | bytes 524288 | tf_op jit(solution)/shard_map/psum | solution.py:51
  84.4 156.6 %all-gather.3.cloned.1.call-start = ((), (), s32[]{:S(2)}) async-start(), calls=%async_computation.5 | async-start | bytes 5242880 | tf_op jit(solution)/shard_map/all_gather | solution.py:63
  153.5 0.8 copy-start.4
  157.2 7.5 %copy-start.5 = (f32[512,128]{0,1:T(8,128)S(1)}, f32[512,128]{0,1:T(8,128)}, u32[]{:S(2)}) copy-start(f32[512,128]{0,1:T(8,128)} %get-tuple-element.25) | copy-start | bytes 786436
Sparse Core Ops, SparseCore 0:
  28.5 46.3 reduce-scatter.2
  77.2 7.1 reduce-scatter.4
  87.3 44.1 all-reduce.1
  163.0 77.9 all-gather.2
